TPU v7x, 32 devices: a whole 2x2x4 slice. The times are simulated.
32 devices in a mesh: fs: 8 (over z, x), tp: 4 (over y, core).
Axes of the slice: x: 2, y: 2, z: 4, core: 2. Of those that a mesh axis runs over, the one named last changes fastest.
Arguments:
- layer_input: bfloat16 [6144, 2048], P('fs'), may hold values from -6 to 6
- branch_cotangent: bfloat16 [6144, 1024], P('fs', 'tp'), may hold values from -0.057373047 to 0.057373047
- gate_cotangent: bfloat16 [6144, 1024], P('fs', 'tp'), may hold values from -0.057373047 to 0.057373047
- branch_factor: bfloat16 [2048, 128], P('fs'), may hold values from -0.5 to 0.5
- gate_factor: bfloat16 [2048, 128], P('fs'), may hold values from -0.5 to 0.5
- branch_weight: float32 [2048, 1024], P('fs', 'tp'), may hold values from -6 to 6
- gate_weight: float32 [2048, 1024], P('fs', 'tp'), may hold values from -6 to 6
- branch_first: float32 [128, 1024], P(None, 'tp'), may hold values from -6 to 6
- gate_first: float32 [128, 1024], P(None, 'tp'), may hold values from -6 to 6
- branch_second: float32 [128, 1024], P(None, 'tp'), may hold values from 0.0625 to 900
- gate_second: float32 [128, 1024], P(None, 'tp'), may hold values from 0.0625 to 900
Outputs:
- branch_step: float32 [2048, 1024], P('fs', 'tp')
- gate_step: float32 [2048, 1024], P('fs', 'tp')
- branch_new: float32 [2048, 1024], P('fs', 'tp')
- gate_new: float32 [2048, 1024], P('fs', 'tp')
- branch_copy: bfloat16 [2048, 1024], P(None, 'tp')
- gate_copy: bfloat16 [2048, 1024], P(None, 'tp')
- branch_first_new: float32 [128, 1024], P(None, 'tp')
- gate_first_new: float32 [128, 1024], P(None, 'tp')
- branch_second_new: float32 [128, 1024], P(None, 'tp')
- gate_second_new: float32 [128, 1024], P(None, 'tp')
All inputs are finite; a program needn't handle non-finite values.
Results may differ from a plain program's by a relative error of at most 0.00055.
Values may be sent and summed in bfloat16 or wider, within the bound.
A program may use at most 64 MiB of HBM per device.

v0:
```python
import jax
import jax.numpy as jnp
from jax import lax
from jax.sharding import PartitionSpec as P

first_decay = 0.8
second_decay = 0.9
learn_rate = 0.5


def update_moments(projected, first_old, second_old):
    first_new = first_decay * first_old + (1.0 - first_decay) * projected
    second_new = second_decay * second_old + (1.0 - second_decay) * projected * projected
    return (first_new, second_new, first_new / jnp.sqrt(second_new))


def local(
    layer_input,
    branch_cotangent,
    gate_cotangent,
    branch_factor,
    gate_factor,
    branch_weight,
    gate_weight,
    branch_first,
    gate_first,
    branch_second,
    gate_second,
):
    highest = lax.Precision.HIGHEST
    width = branch_cotangent.shape[1]
    branch_whole, gate_whole = (
        lax.all_gather(branch_factor, "fs", axis=0, tiled=True),
        lax.all_gather(gate_factor, "fs", axis=0, tiled=True),
    )
    branch_rows = jnp.dot(layer_input, branch_whole, preferred_element_type=jnp.float32)
    gate_rows = jnp.dot(layer_input, gate_whole, preferred_element_type=jnp.float32)
    branch_local = jnp.einsum(
        "tr,tw->rw", branch_rows, branch_cotangent.astype(jnp.float32), precision=highest
    )
    gate_local = jnp.einsum(
        "tr,tw->rw", gate_rows, gate_cotangent.astype(jnp.float32), precision=highest
    )
    branch_projected, gate_projected = lax.psum((branch_local, gate_local), "fs")
    branch_first_new, branch_second_new, branch_direction = update_moments(
        branch_projected, branch_first, branch_second
    )
    gate_first_new, gate_second_new, gate_direction = update_moments(
        gate_projected, gate_first, gate_second
    )
    local_squares = jnp.sum(branch_direction * branch_direction) + jnp.sum(
        gate_direction * gate_direction
    )
    sum_squares = lax.psum(local_squares, "tp")
    entries = 2 * branch_direction.shape[0] * width * lax.axis_size("tp")
    step_scale = learn_rate / jnp.sqrt(sum_squares / entries + 1e-06)
    branch_step = -step_scale * jnp.dot(
        branch_factor.astype(jnp.float32), branch_direction, precision=highest
    )
    gate_step = -step_scale * jnp.dot(
        gate_factor.astype(jnp.float32), gate_direction, precision=highest
    )
    branch_new = branch_weight + branch_step
    gate_new = gate_weight + gate_step
    branch_copy, gate_copy = (
        lax.all_gather(branch_new.astype(jnp.bfloat16), "fs", axis=0, tiled=True),
        lax.all_gather(gate_new.astype(jnp.bfloat16), "fs", axis=0, tiled=True),
    )
    return (
        branch_step,
        gate_step,
        branch_new,
        gate_new,
        branch_copy,
        gate_copy,
        branch_first_new,
        gate_first_new,
        branch_second_new,
        gate_second_new,
    )


def solution(mesh):
    return jax.shard_map(
        local,
        mesh=mesh,
        in_specs=(
            P("fs", None),
            P("fs", "tp"),
            P("fs", "tp"),
            P("fs", None),
            P("fs", None),
            P("fs", "tp"),
            P("fs", "tp"),
            P(None, "tp"),
            P(None, "tp"),
            P(None, "tp"),
            P(None, "tp"),
        ),
        out_specs=(
            P("fs", "tp"),
            P("fs", "tp"),
            P("fs", "tp"),
            P("fs", "tp"),
            P(None, "tp"),
            P(None, "tp"),
            P(None, "tp"),
            P(None, "tp"),
            P(None, "tp"),
            P(None, "tp"),
        ),
        check_vma=False,
    )
```

profile of v0, /device:TPU:0, one launch (start us, length us, event | category | flops | bytes accessed | tf_op | source)
XLA Modules:
  0.0 251.8 jit_solution(14178861783154490260)
XLA Ops:
  7.2 0.0 all-reduce.3.cloned.1.call-start
  7.2 33.4 %all_gather.12 = bf16[2048,128]{1,0:T(8,128)(2,1)S(1)} all-gather(bf16[256,128]{1,0:T(8,128)(2,1)} %param.14), channel_id=1, replica_groups=mesh['fs'=8,'tp'=4] {'fs'}, dimensions={0}, use_global_device_ids=true | all-gather | bytes 589824 | tf_op jit(solution)/shard_map/all_gather | solution.py:33
  40.6 31.4 %all_gather.13 = bf16[2048,128]{1,0:T(8,128)(2,1)S(1)} all-gather(bf16[256,128]{1,0:T(8,128)(2,1)} %param.15), channel_id=1, replica_groups=mesh['fs'=8,'tp'=4] {'fs'}, dimensions={0}, use_global_device_ids=true | all-gather | bytes 589824 | tf_op jit(solution)/shard_map/all_gather | solution.py:34
  72.0 1.0 fusion.8
  73.0 1.0 fusion.10
  74.0 1.1 fusion.9
  75.2 1.1 fusion.11
  76.3 0.0 all-gather.5.cloned.1.call-start
  76.4 72.8 %all-reduce.3.cloned.1.call-done = (f32[128,256]{1,0:T(8,128)}, f32[128,256]{1,0:T(8,128)}) async-done(((f32[128,256]{1,0:T(8,128)}, f32[128,256]{1,0:T(8,128)}), (f32[128,256]{1,0:T(8,128)}, f32[128,256]{1,0:T(8,128)})) %all-reduce.3.cloned.1.call-update) | async-done | bytes 262160 | tf_op jit(solution)/shard_map/psum | solution.py:44
  149.1 2.6 %multiply_reduce_fusion = (f32[]{:T(128)}, f32[128,256]{1,0:T(8,128)S(1)}, f32[128,256]{1,0:T(8,128)}, f32[]{:T(128)}, f32[128,256]{1,0:T(8,128)}, /*index=5*/f32[128,256]{1,0:T(8,128)}) fusion(f32[128,256]{1,0:T(8,128)} %get-tuple-element.21, f32[128,256]{1,0:T(8,128)} %param.21, f32[128,256]{1,0:T(8,128)} %param.19, f32[128,256]{1,0:T(8,128)} %get-tuple-element.20, ...), kind=kLoop, calls=%fused_computation.8 | loop fusion | flops 655358 | bytes 1310728 | tf_op jit(solution)/shard_map/reduce_sum | solution.py:51
  153.1 0.8 copy.22
  153.9 6.1 %psum.23 = f32[]{:T(128)} all-reduce(f32[]{:T(128)S(6)} %add.34), channel_id=1, replica_groups=mesh['fs'=8,'tp'=4] {'tp'}, use_global_device_ids=true, to_apply=%region_4.0 | all-reduce | flops 1 | bytes 8 | tf_op jit(solution)/shard_map/psum | solution.py:54
  160.7 2.1 fusion.4
  162.9 0.0 all-gather.3.cloned.1.call-start
  162.9 1.8 copy.21
  164.7 2.3 fusion.5
  167.0 1.8 copy.26
  168.8 0.8 copy.24
  169.6 1.8 copy.25
  171.4 1.8 copy.23
  173.2 28.7 %all-gather.5.cloned.1.call-done = bf16[2048,256]{0,1:T(8,128)(2,1)} async-done(((bf16[256,256]{0,1:T(8,128)(2,1)}), bf16[2048,256]{0,1:T(8,128)(2,1)}) %all-gather.5.cloned.1.call-update) | async-done | bytes 1048592 | tf_op jit(solution)/shard_map/all_gather | solution.py:67
  201.9 2.3 copy.28
  204.2 38.8 %all-gather.3.cloned.1.call-done = bf16[2048,256]{0,1:T(8,128)(2,1)} async-done(((bf16[256,256]{0,1:T(8,128)(2,1)}), bf16[2048,256]{0,1:T(8,128)(2,1)}) %all-gather.3.cloned.1.call-update) | async-done | bytes 1048592 | tf_op jit(solution)/shard_map/all_gather | solution.py:66
  243.0 2.3 copy.27
  (13 shorter events, 0.1 us)
Async XLA Ops:
  7.2 64.8 %copy-start = (bf16[768,2048]{1,0:T(8,128)(2,1)S(1)}, bf16[768,2048]{1,0:T(8,128)(2,1)}, u32[]{:S(2)}) copy-start(bf16[768,2048]{1,0:T(8,128)(2,1)} %param.11) | copy-start | bytes 9437188
  7.2 142.0 %all-reduce.3.cloned.1.call-start = ((), (), s32[]{:S(2)}) async-start(), calls=%async_computation.2 | async-start | bytes 524288 | tf_op jit(solution)/shard_map/psum | solution.py:44
  73.0 1.0 copy-start.2
  73.0 2.2 copy-start.3
  73.0 80.0 %copy-start.4 = (f32[256,256]{1,0:T(8,128)S(1)}, f32[256,256]{1,0:T(8,128)}, u32[]{:S(2)}) copy-start(f32[256,256]{1,0:T(8,128)} %param.17) | copy-start | bytes 786436
  76.3 125.6 %all-gather.5.cloned.1.call-start = ((), (), s32[]{:S(2)}) async-start(), calls=%async_computation.1 | async-start | bytes 1179648 | tf_op jit(solution)/shard_map/all_gather | solution.py:67
  151.7 52.4 %copy-start.1 = (f32[128,256]{1,0:T(8,128)}, f32[128,256]{1,0:T(8,128)S(1)}, u32[]{:S(2)}) copy-start(f32[128,256]{1,0:T(8,128)S(1)} %get-tuple-element.27) | copy-start | bytes 393220
  162.9 80.1 %all-gather.3.cloned.1.call-start = ((), (), s32[]{:S(2)}) async-start(), calls=%async_computation | async-start | bytes 1179648 | tf_op jit(solution)/shard_map/all_gather | solution.py:66
Sparse Core Ops, SparseCore 0:
  76.5 72.6 all-reduce.2
  163.0 38.8 all-gather.4
  204.5 38.3 all-gather.2
where the time goes:
time: 252 us
  waiting for transfers between devices  140 us (56%)
  blocking collectives  70.9 us (28%)
  between operations  15.8 us (6%)
  local copies, waits for them, and re-layouts  13.4 us (5%)
  matrix products  8.61 us (3%)
  other arithmetic  2.6 us (1%)
    psum x1, waiting for transfers between devices, local(): lax.psum((branch_local, gate_local), 'fs')  72.8 us
    all_gather x1, waiting for transfers between devices, local(): lax.all_gather(branch_new.astype(jnp.bfloat16), 'fs', axis=0, tiled=True)  38.8 us
    all_gather x1, blocking collectives, local(): lax.all_gather(branch_factor, 'fs', axis=0, tiled=True)  33.4 us
    all_gather x1, blocking collectives, local(): lax.all_gather(gate_factor, 'fs', axis=0, tiled=True)  31.4 us
    all_gather x1, waiting for transfers between devices, local(): lax.all_gather(gate_new.astype(jnp.bfloat16), 'fs', axis=0, tiled=True)  28.7 us
    unnamed x18, local copies, waits for them, and re-layouts  13.4 us
    psum x1, blocking collectives, local(): sum_squares = lax.psum(local_squares, 'tp')  6.14 us
  transfers between devices with their start and end apart: 3, of which 3 were waited for; matrix products, arithmetic and copies ran while one was open for 5% of the time, Pallas kernels for 0%

commit v1 on v0

--- a/solution.py
+++ b/solution.py
@@ -1,6 +1,10 @@
+import functools
+
 import jax
 import jax.numpy as jnp
 from jax import lax
+from jax.experimental import pallas as pl
+from jax.experimental.pallas import tpu as pltpu
 from jax.sharding import PartitionSpec as P
 
 first_decay = 0.8
@@ -80,9 +84,372 @@
     )
 
 
+BF, F32 = jnp.bfloat16, jnp.float32
+
+
+def parts(value, count):
+    terms = []
+    for _ in range(count):
+        term = value.astype(BF)
+        terms.append(term)
+        value = value - term.astype(F32)
+    return terms
+
+
+def remote(src, dst, send_sem, recv_sem, **where):
+    return pltpu.make_async_remote_copy(
+        src_ref=src,
+        dst_ref=dst,
+        send_sem=send_sem,
+        recv_sem=recv_sem,
+        device_id=where,
+        device_id_type=pl.DeviceIdType.MESH,
+    )
+
+
+class Line:
+    def __init__(self, nf, me, piece, recv, up, down, across):
+        self.nl = nf // 2
+        self.me, self.z, self.x = me, me // 2, me % 2
+        self.piece, self.recv = piece, recv
+        self.sems = {"up": up, "down": down, "across": across}
+
+    def copy(self, slot, way):
+        target = {"up": self.me + 2, "down": self.me - 2, "across": self.me + 1 - 2 * self.x}[way]
+        return remote(self.piece(slot), self.piece(slot), self.sems[way].at[slot], self.recv.at[slot], fs=target)
+
+    def arrive(self, slot):
+        self.copy(slot, "across").wait_recv()
+
+    def open(self):
+        @pl.when(self.z < self.nl - 1)
+        def _():
+            self.copy(self.me, "up").start()
+
+        @pl.when(self.z > 0)
+        def _():
+            self.copy(self.me, "down").start()
+
+        self.copy(self.me, "across").start()
+
+    def step(self, dist, then=lambda slot: None):
+        @pl.when(self.z >= dist)
+        def _():
+            slot = self.me - 2 * dist
+            self.arrive(slot)
+
+            @pl.when(self.z < self.nl - 1)
+            def _():
+                self.copy(slot, "up").start()
+
+            self.copy(slot, "across").start()
+            then(slot)
+
+        @pl.when(self.z + dist < self.nl)
+        def _():
+            slot = self.me + 2 * dist
+            self.arrive(slot)
+
+            @pl.when(self.z > 0)
+            def _():
+                self.copy(slot, "down").start()
+
+            self.copy(slot, "across").start()
+            then(slot)
+
+    def other(self, dist, then=lambda slot: None):
+        pair = self.me + 1 - 2 * self.x
+        if dist == 0:
+            self.arrive(pair)
+            then(pair)
+            return
+
+        @pl.when(self.z >= dist)
+        def _():
+            self.arrive(pair - 2 * dist)
+            then(pair - 2 * dist)
+
+        @pl.when(self.z + dist < self.nl)
+        def _():
+            self.arrive(pair + 2 * dist)
+            then(pair + 2 * dist)
+
+    def close(self):
+        for line in range(self.nl):
+            slot = 2 * line + self.x
+
+            @pl.when((self.z >= line) & (self.z < self.nl - 1))
+            def _():
+                self.copy(slot, "up").wait_send()
+
+            @pl.when((self.z <= line) & (self.z > 0))
+            def _():
+                self.copy(slot, "down").wait_send()
+
+            self.copy(slot, "across").wait_send()
+
+
+def main_kernel(nf, nt, *refs):
+    x_in, c_in, f_in, w_in = refs[0], refs[1:3], refs[3:5], refs[5:7]
+    first_in, second_in = refs[7:9], refs[9:11]
+    step_out, new_out, copy_out, first_out, second_out = (refs[i : i + 2] for i in range(11, 21, 2))
+    (xv, cv, fbuf, rl, rs, rfull, ss, wv, m1, m2, stv, nwv, fnv, snv, cbuf) = refs[21:36]
+    (in_sem, out_sem, f_sem, core_sem, rs_sem, ag_sem, ss_sem, cp_sem, co_sem) = refs[36:]
+    me, tp = lax.axis_index("fs"), lax.axis_index("tp")
+    depth = f_in[0].shape[0]
+    rank = f_in[0].shape[1]
+    half = depth // 2
+    core = tp % 2
+    mate = tp + 1 - 2 * core
+    pr = rs.shape[1]
+
+    def block(slot):
+        return pl.ds(pl.multiple_of(slot * depth, depth), depth)
+
+    loads = [pltpu.make_async_copy(f_in[p], fbuf.at[block(me), pl.ds(p * rank, rank)], in_sem.at[p]) for p in range(2)]
+    loads += [pltpu.make_async_copy(x_in, xv, in_sem.at[2])]
+    for i, (src, dst) in enumerate(((c_in, cv), (first_in, m1), (second_in, m2), (w_in, wv))):
+        loads += [pltpu.make_async_copy(src[p], dst.at[p], in_sem.at[3 + 2 * i + p]) for p in range(2)]
+    for load in loads:
+        load.start()
+
+    barrier = pltpu.get_barrier_semaphore()
+    for k in range(1, nf):
+        pl.semaphore_signal(barrier, inc=1, device_id={"fs": (me + k) % nf}, device_id_type=pl.DeviceIdType.MESH)
+    for k in range(1, nt):
+        pl.semaphore_signal(barrier, inc=1, device_id={"tp": (tp + k) % nt}, device_id_type=pl.DeviceIdType.MESH)
+    pl.semaphore_wait(barrier, nf + nt - 2)
+
+    def half_of(slot, which):
+        return fbuf.at[pl.ds(pl.multiple_of(slot * depth + which * half, half), half), :]
+
+    gather = Line(nf, me, lambda slot: half_of(slot, core), f_sem.at[0], f_sem.at[1], f_sem.at[2], f_sem.at[3])
+
+    def hand(slot):
+        view = half_of(slot, core)
+        return remote(view, view, core_sem.at[0, slot], core_sem.at[1, slot], tp=mate)
+
+    def take(slot):
+        view = half_of(slot, 1 - core)
+        remote(view, view, core_sem.at[0, slot], core_sem.at[1, slot], tp=mate).wait_recv()
+
+    loads[0].wait()
+    loads[1].wait()
+    gather.open()
+    pass_on = lambda slot: hand(slot).start()
+    gather.other(0, pass_on)
+    for dist in range(1, nf // 2):
+        gather.step(dist, pass_on)
+        gather.other(dist, pass_on)
+    for load in loads[2:5]:
+        load.wait()
+    for k in range(1, nf):
+        take((me + k) % nf)
+
+    rows = jnp.dot(xv[...], fbuf[...], preferred_element_type=F32)
+    terms = parts(rows, 2)
+    for p in range(2):
+        total = 0.0
+        for term in terms:
+            total = total + lax.dot_general(
+                term[:, p * rank : (p + 1) * rank], cv[p], (((0,), (0,)), ((), ())), preferred_element_type=F32
+            )
+        rl[p * rank : (p + 1) * rank, :] = total
+
+    def piece(slot):
+        return pl.ds(pl.multiple_of(slot * pr, pr), pr)
+
+    def scatter(k):
+        to = (me + k) % nf
+        return remote(rl.at[piece(to), :], rs.at[me], rs_sem.at[0, k], rs_sem.at[1, me], fs=to)
+
+    for k in range(1, nf):
+        scatter(k).start()
+    summed = rl[piece(me), :]
+    for k in range(1, nf):
+        frm = (me + k) % nf
+        remote(rl.at[piece(me), :], rs.at[frm], rs_sem.at[0, k], rs_sem.at[1, frm], fs=frm).wait_recv()
+        summed = summed + rs[frm]
+    rfull[piece(me), :] = summed
+
+    def spread(k):
+        view = rfull.at[piece(me), :]
+        return remote(view, view, ag_sem.at[0, k], ag_sem.at[1, me], fs=(me + k) % nf)
+
+    for k in range(1, nf):
+        spread(k).start()
+    for load in loads[5:]:
+        load.wait()
+    for k in range(1, nf):
+        frm = (me + k) % nf
+        view = rfull.at[piece(frm), :]
+        remote(view, view, ag_sem.at[0, k], ag_sem.at[1, frm], fs=frm).wait_recv()
+
+    squares = jnp.zeros((), F32)
+    directions = []
+    for p in range(2):
+        projected = rfull[p * rank : (p + 1) * rank, :]
+        first_new, second_new, direction = update_moments(projected, m1[p], m2[p])
+        fnv[p] = first_new
+        snv[p] = second_new
+        squares = squares + jnp.sum(direction * direction)
+        directions.append(direction)
+    ss[tp] = jnp.full(ss.shape[1:], squares, F32)
+
+    def tell(k):
+        return remote(ss.at[tp], ss.at[tp], ss_sem.at[0, k], ss_sem.at[1, tp], tp=(tp + k) % nt)
+
+    for k in range(1, nt):
+        tell(k).start()
+    raw = []
+    for p in range(2):
+        own = fbuf[block(me), p * rank : (p + 1) * rank]
+        total = 0.0
+        for term in reversed(parts(directions[p], 3)):
+            total = total + jnp.dot(own, term, preferred_element_type=F32)
+        raw.append(total)
+    for k in range(1, nt):
+        frm = (tp + k) % nt
+        remote(ss.at[frm], ss.at[frm], ss_sem.at[0, k], ss_sem.at[1, frm], tp=frm).wait_recv()
+    total = ss[0]
+    for t in range(1, nt):
+        total = total + ss[t]
+    entries = 2 * rank * directions[0].shape[1] * nt
+    scale = (learn_rate / jnp.sqrt(total / entries + 1e-06))[0:1, 0:1]
+
+    lines = []
+    for p in range(2):
+        step = -scale * raw[p]
+        stv[p] = step
+        new = wv[p] + step
+        nwv[p] = new
+        cbuf[p, block(me), :] = new.astype(BF)
+        lines.append(
+            Line(
+                nf,
+                me,
+                functools.partial(lambda p, slot: cbuf.at[p, block(slot), :], p),
+                cp_sem.at[p, 0],
+                cp_sem.at[p, 1],
+                cp_sem.at[p, 2],
+                cp_sem.at[p, 3],
+            )
+        )
+        lines[p].open()
+    outs = []
+    for i, (src, dst) in enumerate(((fnv, first_out), (snv, second_out), (stv, step_out), (nwv, new_out))):
+        outs += [pltpu.make_async_copy(src.at[p], dst[p], out_sem.at[2 * i + p]) for p in range(2)]
+    for out in outs:
+        out.start()
+
+    def put(p, slot):
+        return pltpu.make_async_copy(cbuf.at[p, block(slot), :], copy_out[p].at[block(slot), :], co_sem.at[p, slot])
+
+    starts = [functools.partial(lambda p, slot: put(p, slot).start(), p) for p in range(2)]
+    for p in range(2):
+        starts[p](me)
+    for dist in range(1, nf // 2):
+        for p in range(2):
+            lines[p].step(dist, starts[p])
+        for p in range(2):
+            lines[p].other(dist - 1, starts[p])
+    for p in range(2):
+        lines[p].other(nf // 2 - 1, starts[p])
+
+    gather.close()
+    for line in lines:
+        line.close()
+    for k in range(1, nf):
+        hand((me + k) % nf).wait_send()
+        scatter(k).wait_send()
+        spread(k).wait_send()
+    for k in range(1, nt):
+        tell(k).wait_send()
+    for out in outs:
+        out.wait()
+    for p in range(2):
+        for slot in range(nf):
+            put(p, slot).wait()
+
+
+def out_kernel(n, *refs):
+    srcs, dsts, bufs, sems = refs[:n], refs[n : 2 * n], refs[2 * n : 3 * n], refs[3 * n]
+    for i in range(n):
+        pltpu.make_async_copy(srcs[i], bufs[i], sems.at[0, i]).start()
+    for i in range(n):
+        pltpu.make_async_copy(srcs[i], bufs[i], sems.at[0, i]).wait()
+        pltpu.make_async_copy(bufs[i], dsts[i], sems.at[1, i]).start()
+    for i in range(n):
+        pltpu.make_async_copy(bufs[i], dsts[i], sems.at[1, i]).wait()
+
+
+def fused(nf, nt, *args):
+    x, cot, factor, weight, first = args[0], args[1], args[3], args[5], args[7]
+    tokens, width = cot.shape
+    depth, rank = factor.shape
+    pr = 2 * rank // nf
+    shape = jax.ShapeDtypeStruct
+    outs = [shape(weight.shape, F32)] * 4 + [shape((nf * depth, width), BF)] * 2 + [shape(first.shape, F32)] * 4
+    anywhere = pl.BlockSpec(memory_space=pl.ANY)
+    vmem, dma = pltpu.VMEM, pltpu.SemaphoreType.DMA
+    results = pl.pallas_call(
+        functools.partial(main_kernel, nf, nt),
+        out_shape=outs,
+        in_specs=[anywhere] * 11,
+        out_specs=[anywhere] * 10,
+        scratch_shapes=[
+            vmem(x.shape, BF),
+            vmem((2, tokens, width), BF),
+            vmem((nf * depth, 2 * rank), BF),
+            vmem((2 * rank, width), F32),
+            vmem((nf, pr, width), F32),
+            vmem((2 * rank, width), F32),
+            vmem((nt, 8, 128), F32),
+            vmem((2, depth, width), F32),
+            vmem((2, rank, width), F32),
+            vmem((2, rank, width), F32),
+            vmem((2, depth, width), F32),
+            vmem((2, depth, width), F32),
+            vmem((2, rank, width), F32),
+            vmem((2, rank, width), F32),
+            vmem((2, nf * depth, width), BF),
+            dma((11,)),
+            dma((8,)),
+            dma((4, nf)),
+            dma((2, nf)),
+            dma((2, nf)),
+            dma((2, nf)),
+            dma((2, nt)),
+            dma((2, 4, nf)),
+            dma((2, nf)),
+        ],
+        compiler_params=pltpu.CompilerParams(
+            collective_id=0, has_side_effects=True, vmem_limit_bytes=40 * 1024 * 1024
+        ),
+    )(*args)
+    return pl.pallas_call(
+        functools.partial(out_kernel, len(outs)),
+        out_shape=outs,
+        in_specs=[anywhere] * 10,
+        out_specs=[anywhere] * 10,
+        scratch_shapes=[vmem(o.shape, o.dtype) for o in outs] + [dma((2, len(outs)))],
+    )(*results)
+
+
+def fits(nf, nt, depth, rank):
+    return nf % 2 == 0 and nt % 2 == 0 and nf <= 16 and depth % 32 == 0 and (2 * rank) % (8 * nf) == 0
+
+
+def device_step(nf, nt, *args):
+    depth, rank = args[3].shape
+    if fits(nf, nt, depth, rank):
+        return tuple(fused(nf, nt, *args))
+    return local(*args)
+
+
 def solution(mesh):
     return jax.shard_map(
-        local,
+        functools.partial(device_step, mesh.shape["fs"], mesh.shape["tp"]),
         mesh=mesh,
         in_specs=(
             P("fs", None),

time: 252 us -> 89.3 us (0.35)
  waiting for transfers between devices: 140 us -> 0 us
  blocking collectives: 70.9 us -> 0 us
  Pallas kernels: 0 us -> 69.7 us
  between operations: 15.8 us -> 0.69 us
  matrix products: 8.61 us -> 0 us
  local copies, waits for them, and re-layouts: 13.4 us -> 18.4 us
  other arithmetic: 2.6 us -> 0 us
    psum x1 -> x0, waiting for transfers between devices: 72.8 us -> none  [local(): lax.psum((branch_local, gate_local), 'fs')]
    pallas_call x0 -> x2, Pallas kernels: none -> 69.7 us  [the longest x1 66.5 us: fused(): pl.pallas_call(functools.partial(main_kernel, nf, nt), out_shape=outs, in...]
    all_gather x2 -> x0, waiting for transfers between devices: 67.5 us -> none  [the longest x1 38.8 us: local(): lax.all_gather(branch_new.astype(jnp.bfloat16), 'fs', axis=0, tiled=True)]
    all_gather x2 -> x0, blocking collectives: 64.8 us -> none  [the longest x1 33.4 us: local(): lax.all_gather(branch_factor, 'fs', axis=0, tiled=True)]
    dot_general x6 -> x0, matrix products: 8.61 us -> none  [the longest x1 2.26 us: local(): jnp.dot(branch_factor.astype(jnp.float32), branch_direction, precision=hi...]
    psum x1 -> x0, blocking collectives: 6.14 us -> none  [local(): sum_squares = lax.psum(local_squares, 'tp')]
    unnamed x18 -> x42, local copies, waits for them, and re-layouts: 13.4 us -> 18.4 us
    reduce_sum x1 -> x0, other arithmetic: 2.6 us -> none  [local(): jnp.sum(gate_direction * gate_direction)]
  transfers between devices with their start and end apart: 3 -> 0, of which waited for: 3 -> 0; matrix products, arithmetic and copies ran while one was open for 5% -> 0% of each run, Pallas kernels for 0% -> 0%
where the time goes in v1:
time: 89.3 us; the launch traced here: 88.8 us
  Pallas kernels  69.7 us (78%)
  local copies, waits for them, and re-layouts  18.4 us (21%)
    pallas_call x1, Pallas kernels, fused(): pl.pallas_call(functools.partial(main_kernel, nf, nt), out_shape=outs, in...  66.5 us
    unnamed x42, local copies, waits for them, and re-layouts  18.4 us
    pallas_call x1, Pallas kernels, fused(): pl.pallas_call(functools.partial(out_kernel, len(outs)), out_shape=outs,...  3.2 us

profile of v1, /device:TPU:0, one launch (start us, length us, event | category | flops | bytes accessed | tf_op | source)
XLA Modules:
  0.0 88.8 jit_solution(12366245733309264723)
XLA Ops:
  0.6 0.0 copy-start
  0.7 1.9 %copy-done = bf16[768,2048]{1,0:T(8,128)(2,1)S(1)} copy-done((bf16[768,2048]{1,0:T(8,128)(2,1)S(1)}, bf16[768,2048]{1,0:T(8,128)(2,1)}, u32[]{:S(2)}) %copy-start) | copy-done | bytes 3145752
  2.5 1.0 %copy-done.3 = bf16[768,256]{1,0:T(8,128)(2,1)S(1)} copy-done((bf16[768,256]{1,0:T(8,128)(2,1)S(1)}, bf16[768,256]{1,0:T(8,128)(2,1)}, u32[]{:S(2)}) %copy-start.3) | copy-done | bytes 393240
  3.5 1.0 %copy-done.4 = bf16[768,256]{1,0:T(8,128)(2,1)S(1)} copy-done((bf16[768,256]{1,0:T(8,128)(2,1)S(1)}, bf16[768,256]{1,0:T(8,128)(2,1)}, u32[]{:S(2)}) %copy-start.4) | copy-done | bytes 393240
  4.5 0.9 %copy-done.9 = f32[256,256]{1,0:T(8,128)S(1)} copy-done((f32[256,256]{1,0:T(8,128)S(1)}, f32[256,256]{1,0:T(8,128)}, u32[]{:S(2)}) %copy-start.9) | copy-done | bytes 262168
  5.5 0.9 %copy-done.10 = f32[256,256]{1,0:T(8,128)S(1)} copy-done((f32[256,256]{1,0:T(8,128)S(1)}, f32[256,256]{1,0:T(8,128)}, u32[]{:S(2)}) %copy-start.10) | copy-done | bytes 262168
  6.4 0.9 %copy-done.11 = f32[128,256]{1,0:T(8,128)S(1)} copy-done((f32[128,256]{1,0:T(8,128)S(1)}, f32[128,256]{1,0:T(8,128)}, u32[]{:S(2)}) %copy-start.11) | copy-done | bytes 131096
  7.3 0.9 %copy-done.12 = f32[128,256]{1,0:T(8,128)S(1)} copy-done((f32[128,256]{1,0:T(8,128)S(1)}, f32[128,256]{1,0:T(8,128)}, u32[]{:S(2)}) %copy-start.12) | copy-done | bytes 131096
  8.2 0.9 %copy-done.13 = f32[128,256]{1,0:T(8,128)S(1)} copy-done((f32[128,256]{1,0:T(8,128)S(1)}, f32[128,256]{1,0:T(8,128)}, u32[]{:S(2)}) %copy-start.13) | copy-done | bytes 131096
  9.1 0.9 %copy-done.14 = f32[128,256]{1,0:T(8,128)S(1)} copy-done((f32[128,256]{1,0:T(8,128)S(1)}, f32[128,256]{1,0:T(8,128)}, u32[]{:S(2)}) %copy-start.14) | copy-done | bytes 131096
  10.1 0.8 copy-done.19
  10.9 0.8 copy-done.20
  11.7 66.5 %shard_map.186 = (f32[256,256]{1,0:T(8,128)S(1)}, f32[256,256]{1,0:T(8,128)S(1)}, f32[256,256]{1,0:T(8,128)S(1)}, f32[256,256]{1,0:T(8,128)S(1)}, bf16[2048,256]...) custom-call(bf16[768,2048]{1,0:T(8,128)(2,1)S(1)} %copy-done, ...), custom_call_target="tpu_custom_call" | custom-call | tf_op jit(solution)/shard_map/pallas_call | solution.py:395
  78.3 1.0 %copy-done.1 = bf16[2048,256]{1,0:T(8,128)(2,1)} copy-done((bf16[2048,256]{1,0:T(8,128)(2,1)}, bf16[2048,256]{1,0:T(8,128)(2,1)S(1)}, u32[]{:S(2)}) %copy-start.1) | copy-done | bytes 1048600
  79.3 1.0 %copy-done.2 = bf16[2048,256]{1,0:T(8,128)(2,1)} copy-done((bf16[2048,256]{1,0:T(8,128)(2,1)}, bf16[2048,256]{1,0:T(8,128)(2,1)S(1)}, u32[]{:S(2)}) %copy-start.2) | copy-done | bytes 1048600
  80.2 0.7 copy-done.5
  80.9 0.7 copy-done.6
  81.6 0.7 copy-done.7
  82.4 0.7 copy-done.8
  83.1 0.6 copy-done.15
  83.7 0.6 copy-done.16
  84.3 0.6 copy-done.17
  85.0 0.6 copy-done.18
  85.6 3.2 %shard_map.187 = (f32[256,256]{1,0:T(8,128)}, f32[256,256]{1,0:T(8,128)}, f32[256,256]{1,0:T(8,128)}, f32[256,256]{1,0:T(8,128)}, bf16[2048,256]{1,0:T(8,128)(2,...) custom-call(f32[256,256]{1,0:T(8,128)} %copy-done.5, ...), custom_call_target="tpu_custom_call" | custom-call | tf_op jit(solution)/shard_map/pallas_call | solution.py:430
  (20 shorter events, 0.0 us)
Async XLA Ops:
  0.6 1.9 %copy-start = (bf16[768,2048]{1,0:T(8,128)(2,1)S(1)}, bf16[768,2048]{1,0:T(8,128)(2,1)}, u32[]{:S(2)}) copy-start(bf16[768,2048]{1,0:T(8,128)(2,1)} %refs_0_.1) | copy-start | bytes 9437188
  2.5 1.0 %copy-start.3 = (bf16[768,256]{1,0:T(8,128)(2,1)S(1)}, bf16[768,256]{1,0:T(8,128)(2,1)}, u32[]{:S(2)}) copy-start(bf16[768,256]{1,0:T(8,128)(2,1)} %refs_1_.1) | copy-start | bytes 1179652
  3.5 1.0 %copy-start.4 = (bf16[768,256]{1,0:T(8,128)(2,1)S(1)}, bf16[768,256]{1,0:T(8,128)(2,1)}, u32[]{:S(2)}) copy-start(bf16[768,256]{1,0:T(8,128)(2,1)} %refs_2_.1) | copy-start | bytes 1179652
  4.5 0.9 %copy-start.9 = (f32[256,256]{1,0:T(8,128)S(1)}, f32[256,256]{1,0:T(8,128)}, u32[]{:S(2)}) copy-start(f32[256,256]{1,0:T(8,128)} %refs_5_.1) | copy-start | bytes 786436
  5.5 0.9 %copy-start.10 = (f32[256,256]{1,0:T(8,128)S(1)}, f32[256,256]{1,0:T(8,128)}, u32[]{:S(2)}) copy-start(f32[256,256]{1,0:T(8,128)} %refs_6_.1) | copy-start | bytes 786436
  6.4 0.9 %copy-start.11 = (f32[128,256]{1,0:T(8,128)S(1)}, f32[128,256]{1,0:T(8,128)}, u32[]{:S(2)}) copy-start(f32[128,256]{1,0:T(8,128)} %refs_7_.1) | copy-start | bytes 393220
  7.3 0.9 %copy-start.12 = (f32[128,256]{1,0:T(8,128)S(1)}, f32[128,256]{1,0:T(8,128)}, u32[]{:S(2)}) copy-start(f32[128,256]{1,0:T(8,128)} %refs_8_.1) | copy-start | bytes 393220
  8.2 0.9 %copy-start.13 = (f32[128,256]{1,0:T(8,128)S(1)}, f32[128,256]{1,0:T(8,128)}, u32[]{:S(2)}) copy-start(f32[128,256]{1,0:T(8,128)} %refs_9_.1) | copy-start | bytes 393220
  9.1 0.9 %copy-start.14 = (f32[128,256]{1,0:T(8,128)S(1)}, f32[128,256]{1,0:T(8,128)}, u32[]{:S(2)}) copy-start(f32[128,256]{1,0:T(8,128)} %refs_10_.1) | copy-start | bytes 393220
  10.1 0.8 copy-start.19
  10.9 0.8 copy-start.20
  78.3 1.0 %copy-start.1 = (bf16[2048,256]{1,0:T(8,128)(2,1)}, bf16[2048,256]{1,0:T(8,128)(2,1)S(1)}, u32[]{:S(2)}) copy-start(bf16[2048,256]{1,0:T(8,128)(2,1)S(1)} %get-tuple-element.24.refs_4_) | copy-start | bytes 3145732
  79.3 1.0 %copy-start.2 = (bf16[2048,256]{1,0:T(8,128)(2,1)}, bf16[2048,256]{1,0:T(8,128)(2,1)S(1)}, u32[]{:S(2)}) copy-start(bf16[2048,256]{1,0:T(8,128)(2,1)S(1)} %get-tuple-element.25.refs_5_) | copy-start | bytes 3145732
  80.2 0.7 copy-start.5
  80.9 0.7 copy-start.6
  81.6 0.7 copy-start.7
  82.4 0.7 copy-start.8
  83.0 0.6 copy-start.15
  83.7 0.6 copy-start.16
  84.3 0.7 copy-start.17
  85.0 0.6 copy-start.18

commit v2 on v1

--- a/solution.py
+++ b/solution.py
@@ -373,14 +373,11 @@
 
 
 def out_kernel(n, *refs):
-    srcs, dsts, bufs, sems = refs[:n], refs[n : 2 * n], refs[2 * n : 3 * n], refs[3 * n]
-    for i in range(n):
-        pltpu.make_async_copy(srcs[i], bufs[i], sems.at[0, i]).start()
-    for i in range(n):
-        pltpu.make_async_copy(srcs[i], bufs[i], sems.at[0, i]).wait()
-        pltpu.make_async_copy(bufs[i], dsts[i], sems.at[1, i]).start()
-    for i in range(n):
-        pltpu.make_async_copy(bufs[i], dsts[i], sems.at[1, i]).wait()
+    copies = [pltpu.make_async_copy(refs[i], refs[n + i], refs[2 * n].at[i]) for i in range(n)]
+    for copy in copies:
+        copy.start()
+    for copy in copies:
+        copy.wait()
 
 
 def fused(nf, nt, *args):
@@ -390,12 +387,12 @@
     pr = 2 * rank // nf
     shape = jax.ShapeDtypeStruct
     outs = [shape(weight.shape, F32)] * 4 + [shape((nf * depth, width), BF)] * 2 + [shape(first.shape, F32)] * 4
-    anywhere = pl.BlockSpec(memory_space=pl.ANY)
+    anywhere, hbm = pl.BlockSpec(memory_space=pl.ANY), pl.BlockSpec(memory_space=pltpu.HBM)
     vmem, dma = pltpu.VMEM, pltpu.SemaphoreType.DMA
     results = pl.pallas_call(
         functools.partial(main_kernel, nf, nt),
         out_shape=outs,
-        in_specs=[anywhere] * 11,
+        in_specs=[hbm] * 11,
         out_specs=[anywhere] * 10,
         scratch_shapes=[
             vmem(x.shape, BF),
@@ -424,15 +421,16 @@
             dma((2, nf)),
         ],
         compiler_params=pltpu.CompilerParams(
-            collective_id=0, has_side_effects=True, vmem_limit_bytes=40 * 1024 * 1024
+            collective_id=0, has_side_effects=True, vmem_limit_bytes=24 * 1024 * 1024
         ),
-    )(*args)
+    )(*[pltpu.with_memory_space_constraint(a, pltpu.HBM) for a in args])
     return pl.pallas_call(
         functools.partial(out_kernel, len(outs)),
         out_shape=outs,
         in_specs=[anywhere] * 10,
-        out_specs=[anywhere] * 10,
-        scratch_shapes=[vmem(o.shape, o.dtype) for o in outs] + [dma((2, len(outs)))],
+        out_specs=[hbm] * 10,
+        scratch_shapes=[dma((len(outs),))],
+        compiler_params=pltpu.CompilerParams(vmem_limit_bytes=1024 * 1024),
     )(*results)
 
 

time: 89.3 us -> 67.9 us (0.76)
  local copies, waits for them, and re-layouts: 18.4 us -> 0 us
  Pallas kernels: 69.7 us -> 67.1 us
    unnamed x42 -> x0, local copies, waits for them, and re-layouts: 18.4 us -> none
    pallas_call x1, Pallas kernels: 66.5 us -> 65.2 us  [fused(): pl.pallas_call(functools.partial(main_kernel, nf, nt), out_shape=outs, in...]
    pallas_call x1, Pallas kernels: 3.2 us -> 1.92 us  [fused(): pl.pallas_call(functools.partial(out_kernel, len(outs)), out_shape=outs,...]
where the time goes in v2:
time: 67.9 us; the launch traced here: 67.7 us
  Pallas kernels  67.1 us (99%)
    pallas_call x1, Pallas kernels, fused(): pl.pallas_call(functools.partial(main_kernel, nf, nt), out_shape=outs, in...  65.2 us
    pallas_call x1, Pallas kernels, fused(): pl.pallas_call(functools.partial(out_kernel, len(outs)), out_shape=outs,...  1.92 us

profile of v2, /device:TPU:0, one launch (start us, length us, event | category | flops | bytes accessed | tf_op | source)
XLA Modules:
  0.0 67.7 jit_solution(2220603050255879223)
XLA Ops:
  0.6 65.2 %shard_map.186 = (f32[256,256]{1,0:T(8,128)S(1)}, f32[256,256]{1,0:T(8,128)S(1)}, f32[256,256]{1,0:T(8,128)S(1)}, f32[256,256]{1,0:T(8,128)S(1)}, bf16[2048,256]...) custom-call(bf16[768,2048]{1,0:T(8,128)(2,1)} %refs_0_.1, ...), custom_call_target="tpu_custom_call" | custom-call | tf_op jit(solution)/shard_map/pallas_call | solution.py:392
  65.8 1.9 %shard_map.187 = (f32[256,256]{1,0:T(8,128)}, f32[256,256]{1,0:T(8,128)}, f32[256,256]{1,0:T(8,128)}, f32[256,256]{1,0:T(8,128)}, bf16[2048,256]{1,0:T(8,128)(2,...) custom-call(f32[256,256]{1,0:T(8,128)S(1)} %get-tuple-element.20.ref, ...), custom_call_target="tpu_custom_call" | custom-call | tf_op jit(solution)/shard_map/pallas_call | solution.py:427

commit v3 on v2

--- a/solution.py
+++ b/solution.py
@@ -85,6 +85,7 @@
 
 
 BF, F32 = jnp.bfloat16, jnp.float32
+SPLIT = 2
 
 
 def parts(value, count):
@@ -108,29 +109,33 @@
 
 
 class Line:
-    def __init__(self, nf, me, piece, recv, up, down, across):
+    def __init__(self, nf, me, own, piece, recv, up, down, across, shift=False):
         self.nl = nf // 2
+        self.own, self.shift = own, shift
         self.me, self.z, self.x = me, me // 2, me % 2
         self.piece, self.recv = piece, recv
         self.sems = {"up": up, "down": down, "across": across}
 
     def copy(self, slot, way):
         target = {"up": self.me + 2, "down": self.me - 2, "across": self.me + 1 - 2 * self.x}[way]
-        return remote(self.piece(slot), self.piece(slot), self.sems[way].at[slot], self.recv.at[slot], fs=target)
+        src = self.own if slot is self.me else self.piece(slot)
+        return remote(src, self.piece(slot), self.sems[way].at[slot], self.recv.at[slot], fs=target)
 
     def arrive(self, slot):
         self.copy(slot, "across").wait_recv()
 
+    def both(self, slot, act):
+        @pl.when(self.z < self.nl - 1)
+        def _():
+            act(self.copy(slot, "up"))
+
+        @pl.when(self.z > 0)
+        def _():
+            act(self.copy(slot, "down"))
+
     def open(self):
-        @pl.when(self.z < self.nl - 1)
-        def _():
-            self.copy(self.me, "up").start()
-
-        @pl.when(self.z > 0)
-        def _():
-            self.copy(self.me, "down").start()
-
         self.copy(self.me, "across").start()
+        self.both(self.me, lambda copy: copy.start())
 
     def step(self, dist, then=lambda slot: None):
         @pl.when(self.z >= dist)
@@ -142,7 +147,8 @@
             def _():
                 self.copy(slot, "up").start()
 
-            self.copy(slot, "across").start()
+            if not (self.shift and dist == 1):
+                self.copy(slot, "across").start()
             then(slot)
 
         @pl.when(self.z + dist < self.nl)
@@ -154,13 +160,16 @@
             def _():
                 self.copy(slot, "down").start()
 
-            self.copy(slot, "across").start()
+            if not (self.shift and dist == 1):
+                self.copy(slot, "across").start()
             then(slot)
 
     def other(self, dist, then=lambda slot: None):
         pair = self.me + 1 - 2 * self.x
         if dist == 0:
             self.arrive(pair)
+            if self.shift:
+                self.both(pair, lambda copy: copy.start())
             then(pair)
             return
 
@@ -186,7 +195,17 @@
             def _():
                 self.copy(slot, "down").wait_send()
 
-            self.copy(slot, "across").wait_send()
+            if self.shift:
+
+                @pl.when((self.z != line - 1) & (self.z != line + 1))
+                def _():
+                    self.copy(slot, "across").wait_send()
+
+            else:
+                self.copy(slot, "across").wait_send()
+
+        if self.shift:
+            self.both(self.me + 1 - 2 * self.x, lambda copy: copy.wait_send())
 
 
 def main_kernel(nf, nt, *refs):
@@ -194,7 +213,7 @@
     first_in, second_in = refs[7:9], refs[9:11]
     step_out, new_out, copy_out, first_out, second_out = (refs[i : i + 2] for i in range(11, 21, 2))
     (xv, cv, fbuf, rl, rs, rfull, ss, wv, m1, m2, stv, nwv, fnv, snv, cbuf) = refs[21:36]
-    (in_sem, out_sem, f_sem, core_sem, rs_sem, ag_sem, ss_sem, cp_sem, co_sem) = refs[36:]
+    (in_sem, out_sem, f_sem, core_sem, rs_sem, ag_sem, ss_sem, cp_sem) = refs[36:]
     me, tp = lax.axis_index("fs"), lax.axis_index("tp")
     depth = f_in[0].shape[0]
     rank = f_in[0].shape[1]
@@ -223,7 +242,7 @@
     def half_of(slot, which):
         return fbuf.at[pl.ds(pl.multiple_of(slot * depth + which * half, half), half), :]
 
-    gather = Line(nf, me, lambda slot: half_of(slot, core), f_sem.at[0], f_sem.at[1], f_sem.at[2], f_sem.at[3])
+    gather = Line(nf, me, half_of(me, core), lambda slot: half_of(slot, core), f_sem.at[0], f_sem.at[1], f_sem.at[2], f_sem.at[3])
 
     def hand(slot):
         view = half_of(slot, core)
@@ -317,44 +336,40 @@
     entries = 2 * rank * directions[0].shape[1] * nt
     scale = (learn_rate / jnp.sqrt(total / entries + 1e-06))[0:1, 0:1]
 
+    cut = depth // SPLIT
+
+    def rows_of(slot, part):
+        return pl.ds(pl.multiple_of(slot * depth + part * cut, cut), cut)
+
     lines = []
     for p in range(2):
         step = -scale * raw[p]
+        new = wv[p] + step
+        cbuf[p] = new.astype(BF)
         stv[p] = step
-        new = wv[p] + step
         nwv[p] = new
-        cbuf[p, block(me), :] = new.astype(BF)
-        lines.append(
-            Line(
-                nf,
-                me,
-                functools.partial(lambda p, slot: cbuf.at[p, block(slot), :], p),
-                cp_sem.at[p, 0],
-                cp_sem.at[p, 1],
-                cp_sem.at[p, 2],
-                cp_sem.at[p, 3],
-            )
-        )
-        lines[p].open()
+        for part in range(SPLIT):
+            i = p * SPLIT + part
+            own = cbuf.at[p, part * cut : (part + 1) * cut, :]
+            piece_of = functools.partial(lambda p, part, slot: copy_out[p].at[rows_of(slot, part), :], p, part)
+            lines.append(Line(nf, me, own, piece_of, *(cp_sem.at[i, j] for j in range(4)), shift=p == 1))
+            lines[i].open()
     outs = []
     for i, (src, dst) in enumerate(((fnv, first_out), (snv, second_out), (stv, step_out), (nwv, new_out))):
         outs += [pltpu.make_async_copy(src.at[p], dst[p], out_sem.at[2 * i + p]) for p in range(2)]
+    for p in range(2):
+        outs += [pltpu.make_async_copy(cbuf.at[p], copy_out[p].at[block(me), :], out_sem.at[8 + p])]
     for out in outs:
         out.start()
-
-    def put(p, slot):
-        return pltpu.make_async_copy(cbuf.at[p, block(slot), :], copy_out[p].at[block(slot), :], co_sem.at[p, slot])
-
-    starts = [functools.partial(lambda p, slot: put(p, slot).start(), p) for p in range(2)]
-    for p in range(2):
-        starts[p](me)
     for dist in range(1, nf // 2):
-        for p in range(2):
-            lines[p].step(dist, starts[p])
-        for p in range(2):
-            lines[p].other(dist - 1, starts[p])
-    for p in range(2):
-        lines[p].other(nf // 2 - 1, starts[p])
+        for line in lines:
+            line.step(dist)
+        if dist == 1:
+            for line in lines:
+                line.other(0)
+    for dist in range(1, nf // 2):
+        for line in lines:
+            line.other(dist)
 
     gather.close()
     for line in lines:
@@ -367,9 +382,6 @@
         tell(k).wait_send()
     for out in outs:
         out.wait()
-    for p in range(2):
-        for slot in range(nf):
-            put(p, slot).wait()
 
 
 def out_kernel(n, *refs):
@@ -409,16 +421,15 @@
             vmem((2, depth, width), F32),
             vmem((2, rank, width), F32),
             vmem((2, rank, width), F32),
-            vmem((2, nf * depth, width), BF),
+            vmem((2, depth, width), BF),
             dma((11,)),
-            dma((8,)),
+            dma((10,)),
             dma((4, nf)),
             dma((2, nf)),
             dma((2, nf)),
             dma((2, nf)),
             dma((2, nt)),
-            dma((2, 4, nf)),
-            dma((2, nf)),
+            dma((2 * SPLIT, 4, nf)),
         ],
         compiler_params=pltpu.CompilerParams(
             collective_id=0, has_side_effects=True, vmem_limit_bytes=24 * 1024 * 1024
@@ -435,7 +446,7 @@
 
 
 def fits(nf, nt, depth, rank):
-    return nf % 2 == 0 and nt % 2 == 0 and nf <= 16 and depth % 32 == 0 and (2 * rank) % (8 * nf) == 0
+    return nf % 2 == 0 and nt % 2 == 0 and nf <= 16 and depth % (16 * SPLIT) == 0 and (2 * rank) % (8 * nf) == 0
 
 
 def device_step(nf, nt, *args):

time: 67.9 us -> 70 us (1.031)
  Pallas kernels: 67.1 us -> 69.2 us
    pallas_call x1, Pallas kernels: 65.2 us -> 67.3 us  [fused(): pl.pallas_call(functools.partial(main_kernel, nf, nt), out_shape=outs, in...]
where the time goes in v3:
time: 70 us; the launch traced here: 69.9 us
  Pallas kernels  69.2 us (99%)
    pallas_call x1, Pallas kernels, fused(): pl.pallas_call(functools.partial(main_kernel, nf, nt), out_shape=outs, in...  67.3 us
    pallas_call x1, Pallas kernels, fused(): pl.pallas_call(functools.partial(out_kernel, len(outs)), out_shape=outs,...  1.92 us

profile of v3, /device:TPU:0, one launch (start us, length us, event | category | flops | bytes accessed | tf_op | source)
XLA Modules:
  0.0 69.9 jit_solution(13087908646187410003)
XLA Ops:
  0.6 67.3 %shard_map.186 = (f32[256,256]{1,0:T(8,128)S(1)}, f32[256,256]{1,0:T(8,128)S(1)}, f32[256,256]{1,0:T(8,128)S(1)}, f32[256,256]{1,0:T(8,128)S(1)}, bf16[2048,256]...) custom-call(bf16[768,2048]{1,0:T(8,128)(2,1)} %refs_0_.1, ...), custom_call_target="tpu_custom_call" | custom-call | tf_op jit(solution)/shard_map/pallas_call | solution.py:404
  67.9 1.9 %shard_map.187 = (f32[256,256]{1,0:T(8,128)}, f32[256,256]{1,0:T(8,128)}, f32[256,256]{1,0:T(8,128)}, f32[256,256]{1,0:T(8,128)}, bf16[2048,256]{1,0:T(8,128)(2,...) custom-call(f32[256,256]{1,0:T(8,128)S(1)} %get-tuple-element.20.ref, ...), custom_call_target="tpu_custom_call" | custom-call | tf_op jit(solution)/shard_map/pallas_call | solution.py:438

commit v4 on v3

--- a/solution.py
+++ b/solution.py
@@ -85,7 +85,7 @@
 
 
 BF, F32 = jnp.bfloat16, jnp.float32
-SPLIT = 2
+SPLIT = 4
 
 
 def parts(value, count):
@@ -361,12 +361,18 @@
         outs += [pltpu.make_async_copy(cbuf.at[p], copy_out[p].at[block(me), :], out_sem.at[8 + p])]
     for out in outs:
         out.start()
+    at_end = (me // 2 == 0) | (me // 2 == nf // 2 - 1)
+
+    def pairs():
+        for line in lines:
+            line.other(0)
+
     for dist in range(1, nf // 2):
         for line in lines:
             line.step(dist)
         if dist == 1:
-            for line in lines:
-                line.other(0)
+            pl.when(at_end)(pairs)
+    pl.when(jnp.logical_not(at_end))(pairs)
     for dist in range(1, nf // 2):
         for line in lines:
             line.other(dist)

time: 70 us -> 68.4 us (0.977)
  Pallas kernels: 69.2 us -> 67.6 us
    pallas_call x1, Pallas kernels: 67.3 us -> 65.6 us  [fused(): pl.pallas_call(functools.partial(main_kernel, nf, nt), out_shape=outs, in...]
where the time goes in v4:
time: 68.4 us; the launch traced here: 68.2 us
  Pallas kernels  67.6 us (99%)
    pallas_call x1, Pallas kernels, fused(): pl.pallas_call(functools.partial(main_kernel, nf, nt), out_shape=outs, in...  65.6 us
    pallas_call x1, Pallas kernels, fused(): pl.pallas_call(functools.partial(out_kernel, len(outs)), out_shape=outs,...  1.92 us

profile of v4, /device:TPU:0, one launch (start us, length us, event | category | flops | bytes accessed | tf_op | source)
XLA Modules:
  0.0 68.2 jit_solution(13778540426649041351)
XLA Ops:
  0.6 65.6 %shard_map.186 = (f32[256,256]{1,0:T(8,128)S(1)}, f32[256,256]{1,0:T(8,128)S(1)}, f32[256,256]{1,0:T(8,128)S(1)}, f32[256,256]{1,0:T(8,128)S(1)}, bf16[2048,256]...) custom-call(bf16[768,2048]{1,0:T(8,128)(2,1)} %refs_0_.1, ...), custom_call_target="tpu_custom_call" | custom-call | tf_op jit(solution)/shard_map/pallas_call | solution.py:410
  66.3 1.9 %shard_map.187 = (f32[256,256]{1,0:T(8,128)}, f32[256,256]{1,0:T(8,128)}, f32[256,256]{1,0:T(8,128)}, f32[256,256]{1,0:T(8,128)}, bf16[2048,256]{1,0:T(8,128)(2,...) custom-call(f32[256,256]{1,0:T(8,128)S(1)} %get-tuple-element.20.ref, ...), custom_call_target="tpu_custom_call" | custom-call | tf_op jit(solution)/shard_map/pallas_call | solution.py:444
